TPU v7x, 256 devices: a whole 4x4x8 slice. The times are simulated.
256 devices in a mesh: ep: 32 (over z, x), tp: 8 (over y, core).
Axes of the slice: x: 4, y: 4, z: 8, core: 2. Of those that a mesh axis runs over, the one named last changes fastest.
Arguments:
- stream: bfloat16 [512, 4096], P(None, 'ep'), may hold values from -6.5 to 6.5
- norm_gain: float32 [4096], P('ep'), may hold values from 0.1 to 1.9
- w_query: bfloat16 [4096, 2048], P('ep', 'tp'), may hold values from -0.09375 to 0.09375
- w_key: bfloat16 [4096, 1024], P('ep', 'tp'), may hold values from -0.09375 to 0.09375
- w_value: bfloat16 [4096, 1024], P('ep', 'tp'), may hold values from -0.09375 to 0.09375
- break_offset: float32 [16], P('tp'), may hold values from -10 to -2
- cache_keys: bfloat16 [512, 1024, 8, 128], P('ep', None, 'tp'), may hold values from -6 to 6
- cache_values: bfloat16 [512, 1024, 8, 128], P('ep', None, 'tp'), may hold values from -6 to 6
- lengths: int32 [512], P('ep'), may hold values from 128 to 1024
- w_output: bfloat16 [2048, 4096], P('tp', 'ep'), may hold values from -0.125 to 0.125
- head_gain: float32 [2048], P('tp'), may hold values from 0.1 to 1.9
- ffn_gain: float32 [4096], P('ep'), may hold values from 0.1 to 1.9
- route_experts: int32 [512, 2], replicated, may hold values from 0 to 31, all different within a row; in each aligned block of 512 rows (0 to 511, 512 to 1023, ...) at most 64 rows name the same one
- route_weights: float32 [512, 2], replicated, may hold values from 0.1 to 1
- expert_gate: bfloat16 [32, 4096, 1024], P('ep', None, 'tp'), may hold values from -0.09375 to 0.09375
- expert_up: bfloat16 [32, 4096, 1024], P('ep', None, 'tp'), may hold values from -0.09375 to 0.09375
- expert_down: bfloat16 [32, 1024, 4096], P('ep', 'tp'), may hold values from -0.1875 to 0.1875
- dense_gate: bfloat16 [4096, 4096], P('ep', 'tp'), may hold values from -0.09375 to 0.09375
- dense_up: bfloat16 [4096, 4096], P('ep', 'tp'), may hold values from -0.09375 to 0.09375
- dense_down: bfloat16 [4096, 4096], P('tp', 'ep'), may hold values from -0.09375 to 0.09375
- mix_gain: float32 [4096], P('ep'), may hold values from 0.1 to 1.9
Outputs:
- mixed_out: bfloat16 [512, 4096], P(None, 'ep')
- key_rows: bfloat16 [512, 1024], P('ep', 'tp')
- value_rows: bfloat16 [512, 1024], P('ep', 'tp')
Inputs may be any that keep to these rules, and one draw needn't show every extreme that they name: `route_experts`: in the whole batch no expert is named by more than 64 pairs, a bound that some block reaches; the 2 experts of a token differ.
All inputs are finite; a program needn't handle non-finite values.
Results may differ from a plain program's by a relative error of at most 0.025.
Values may be sent and summed in bfloat16 or wider, within the bound.
A program may use at most 64 MiB of HBM per device.

v0:
```python
import jax
import jax.numpy as jnp
from jax import lax
from jax.sharding import PartitionSpec as P

EPSILON = 1e-06


def sent_to_all(x, axis):
    size = lax.axis_size(axis)
    return lax.all_to_all(jnp.broadcast_to(x[None], (size, *x.shape)), axis, 0, 0, tiled=True)


def taken_together(x, axis):
    return sent_to_all(x, axis).sum(axis=0)


def split_up(x, dim, size):
    lengths = x.shape
    blocks = x.reshape(*lengths[:dim], size, lengths[dim] // size, *lengths[dim + 1 :])
    return jnp.moveaxis(blocks, dim, 0)


def sent_and_summed(x, axis, dim):
    blocks = split_up(x, dim, lax.axis_size(axis))
    arrived = lax.all_to_all(blocks, axis, split_axis=0, concat_axis=0, tiled=True)
    return arrived.astype(jnp.float32).sum(axis=0)


def joined_along(blocks, dim):
    blocks = jnp.moveaxis(blocks, 0, dim)
    lengths = blocks.shape
    return blocks.reshape(*lengths[:dim], lengths[dim] * lengths[dim + 1], *lengths[dim + 2 :])


def gather_directly(x, axis, dim):
    return joined_along(sent_to_all(x, axis), dim)


def of_everyone(x, axis):
    return sent_to_all(x, axis).astype(jnp.float32).sum(axis=0)


def rms_scale(values, gain_vec, model_width):
    squares = taken_together(jnp.sum(values * values, axis=1), "ep")
    return values * lax.rsqrt(squares / model_width + EPSILON)[:, None] * gain_vec[None, :]


def to_heads(normed, weights):
    return sent_and_summed(
        jnp.dot(normed, weights, preferred_element_type=jnp.float32).astype(jnp.bfloat16), "ep", 0
    )


def from_heads(values, weights):
    partial_value = jnp.dot(
        gather_directly(values, "ep", 0), weights, preferred_element_type=jnp.float32
    )
    return (
        of_everyone(partial_value.astype(jnp.bfloat16), "tp")
        .astype(jnp.float32)
        .astype(jnp.bfloat16)
    )


def expert_terms(inputs, gate_w, up_w, down_w):
    gate_val = jnp.einsum("ecd,edf->ecf", inputs, gate_w, preferred_element_type=jnp.float32)
    up_val = jnp.einsum("ecd,edf->ecf", inputs, up_w, preferred_element_type=jnp.float32)
    hidden = (jax.nn.silu(gate_val) * up_val).astype(jnp.bfloat16)
    return jnp.einsum("ecf,efd->ecd", hidden, down_w, preferred_element_type=jnp.float32)


def slot_table(route_experts, experts, capacity):
    chosen = route_experts.reshape(-1)
    onehot = (chosen[:, None] == jnp.arange(experts, dtype=jnp.int32)[None, :]).astype(jnp.int32)
    earlier = jnp.cumsum(onehot, axis=0) - onehot
    rank_in = jnp.sum(earlier * onehot, axis=1)
    slot_ids = chosen * capacity + rank_in
    owners = jnp.arange(chosen.shape[0], dtype=jnp.int32) // route_experts.shape[1]
    filled = (
        jnp.full((experts * capacity,), route_experts.shape[0], jnp.int32).at[slot_ids].set(owners)
    )
    return (slot_ids, filled)


def per_device(
    stream,
    norm_gain,
    w_query,
    w_key,
    w_value,
    break_offset,
    cache_keys,
    cache_values,
    lengths,
    w_output,
    head_gain,
    ffn_gain,
    route_experts,
    route_weights,
    expert_gate,
    expert_up,
    expert_down,
    dense_gate,
    dense_up,
    dense_down,
    mix_gain,
):
    model_width = stream.shape[1] * lax.axis_size("ep")
    block_width = stream.shape[1]
    seq_count = lengths.shape[0]
    kv_local = cache_keys.shape[2]
    head_dim = cache_keys.shape[3]
    heads_local = break_offset.shape[0]
    group_size = heads_local // kv_local
    cache_len = cache_keys.shape[1]
    streamf = stream.astype(jnp.float32)
    normed = rms_scale(streamf, norm_gain, model_width).astype(jnp.bfloat16)
    projected = to_heads(normed, jnp.concatenate([w_query, w_key, w_value], axis=1))
    q_width = w_query.shape[1]
    k_width = w_key.shape[1]
    queries = (
        projected[:, :q_width]
        .astype(jnp.bfloat16)
        .reshape(seq_count, kv_local, group_size, head_dim)
    )
    key_rows = projected[:, q_width : q_width + k_width].astype(jnp.bfloat16)
    value_rows = projected[:, q_width + k_width :].astype(jnp.bfloat16)
    scores = jnp.einsum("skgd,slkd->skgl", queries, cache_keys, preferred_element_type=jnp.float32)
    scores = (
        scores * head_dim ** (-0.5) + break_offset.reshape(kv_local, group_size)[None, :, :, None]
    )
    in_cache = (jnp.arange(cache_len, dtype=jnp.int32)[None, :] < lengths[:, None])[
        :, None, None, :
    ]
    failed = jnp.where(in_cache, jax.nn.log_sigmoid(-scores), 0.0)
    later_sum = lax.cumsum(failed, axis=3, reverse=True) - failed
    weights = jnp.where(in_cache, jnp.exp(jax.nn.log_sigmoid(scores) + later_sum), 0.0).astype(
        jnp.bfloat16
    )
    attended = jnp.einsum(
        "skgl,slkd->skgd", weights, cache_values, preferred_element_type=jnp.float32
    )
    gains = head_gain.reshape(kv_local, group_size, head_dim)[None]
    normalized = (
        attended * lax.rsqrt(jnp.mean(attended * attended, axis=3, keepdims=True) + EPSILON) * gains
    )
    head_out = normalized.astype(jnp.bfloat16).reshape(seq_count, heads_local * head_dim)
    attn_out = from_heads(head_out, w_output)
    residual = streamf + attn_out.astype(jnp.float32)
    normed_ffn = rms_scale(residual, ffn_gain, model_width).astype(jnp.bfloat16)
    dense_width = dense_gate.shape[1]
    gate_up = to_heads(normed_ffn, jnp.concatenate([dense_gate, dense_up], axis=1))
    dense_hidden = (jax.nn.silu(gate_up[:, :dense_width]) * gate_up[:, dense_width:]).astype(
        jnp.bfloat16
    )
    dense_out = from_heads(dense_hidden, dense_down)
    experts = expert_gate.shape[0] * lax.axis_size("ep")
    capacity = 2 * seq_count * route_experts.shape[1] // expert_gate.shape[0]
    slot_ids, filled = slot_table(route_experts, experts, capacity)
    padded = jnp.concatenate([normed_ffn, jnp.zeros((1, block_width), jnp.bfloat16)], axis=0)
    outgoing = padded[filled].reshape(experts, capacity, block_width)
    slot_share = capacity // lax.axis_size("tp")
    own_slots = lax.dynamic_slice_in_dim(outgoing, lax.axis_index("tp") * slot_share, slot_share, 1)
    arrived = lax.all_to_all(own_slots, "ep", split_axis=0, concat_axis=2, tiled=True)
    gathered = lax.all_gather(arrived, "tp", axis=1, tiled=True)
    partial_value = expert_terms(gathered, expert_gate, expert_up, expert_down)
    summed = sent_and_summed(partial_value.astype(jnp.bfloat16), "tp", 1).astype(jnp.bfloat16)
    came_back = lax.all_to_all(summed, "ep", split_axis=2, concat_axis=0, tiled=True)
    returned = gather_directly(came_back, "tp", 1)
    picked = returned.reshape(experts * capacity, block_width)[slot_ids]
    picked = picked.reshape(route_experts.shape[0], route_experts.shape[1], block_width).astype(
        jnp.float32
    )
    shares = route_weights / jnp.sum(route_weights, axis=1, keepdims=True)
    moe_out = jnp.sum(picked * shares[:, :, None], axis=1)
    mixed_out = (residual + moe_out + mix_gain[None, :] * dense_out.astype(jnp.float32)).astype(
        jnp.bfloat16
    )
    return (mixed_out, key_rows, value_rows)


def solution(mesh):
    in_specs = (
        P(None, "ep"),
        P("ep"),
        P("ep", "tp"),
        P("ep", "tp"),
        P("ep", "tp"),
        P("tp"),
        P("ep", None, "tp", None),
        P("ep", None, "tp", None),
        P("ep"),
        P("tp", "ep"),
        P("tp"),
        P("ep"),
        P(),
        P(),
        P("ep", None, "tp"),
        P("ep", None, "tp"),
        P("ep", "tp", None),
        P("ep", "tp"),
        P("ep", "tp"),
        P("tp", "ep"),
        P("ep"),
    )
    out_specs = (P(None, "ep"), P("ep", "tp"), P("ep", "tp"))
    return jax.shard_map(
        per_device, mesh=mesh, in_specs=in_specs, out_specs=out_specs, check_vma=False
    )
```

profile of v0, /device:TPU:1, one launch (start us, length us, event | category | flops | bytes accessed | tf_op | source)
XLA Modules:
  0.0 309.1 jit_solution(11907331791318313063)
XLA Ops:
  1.8 20.5 %all_to_all.85 = f32[32,1,512]{2,1,0:T(1,128)S(1)} all-to-all(f32[32,1,512]{2,1,0:T(1,128)S(1)} %broadcast_in_dim.37), channel_id=1, replica_groups=mesh['ep'=32,'tp'=8] {'ep'}, dimensions={0} | all-to-all | bytes 131072 | tf_op jit(solution)/shard_map/all_to_all | solution.py:11
  24.5 3.9 %all-to-all-start.1 = ((bf16[32,16,512]{2,1,0:T(8,128)(2,1)}), bf16[32,16,512]{2,1,0:T(8,128)(2,1)S(1)}, u32[]{:S(2)}, u32[]{:S(2)}) async-start(bf16[32,16,512]{2,1,0:T(8,128)(2,1)} %bitcast), calls=%async_computation.1 | async-start | bytes 1048576 | tf_op jit(solution)/shard_map/all_to_all | solution.py:26
  29.1 14.2 %all-to-all-done.1 = bf16[32,16,512]{2,1,0:T(8,128)(2,1)S(1)} async-done(((bf16[32,16,512]{2,1,0:T(8,128)(2,1)}), bf16[32,16,512]{2,1,0:T(8,128)(2,1)S(1)}, u32[]{:S(2)}, u32[]{:S(2)}) %all-to-all-start.1) | async-done | bytes 524320 | tf_op jit(solution)/shard_map/all_to_all | solution.py:26
  47.0 39.6 %reduce-window.14 = f32[16,1,2,8,128]{4,3,2,1,0:T(8,128)S(1)} reduce-window(f32[16,1,2,8,128]{4,3,2,1,0:T(8,128)S(1)} %bitcast.111, f32[]{:T(128)} %constant.52.clone.1), window={size=1x1x1x1x128 pad=0_0x0_0x0_0x0_0x0_127}, to_apply=%region_3.4 | reduce-window | flops 4161536 | bytes 262148 | tf_op jit(solution)/shard_map/reduce-window
  91.3 6.3 %all-to-all-start.2 = ((bf16[32,16,256]{2,1,0:T(8,128)(2,1)}), bf16[32,16,256]{2,1,0:T(8,128)(2,1)S(1)}, u32[]{:S(2)}, u32[]{:S(2)}) async-start(bf16[32,16,256]{2,1,0:T(8,128)(2,1)} %broadcast_in_dim.39), calls=%async_computation.2 | async-start | bytes 524288 | tf_op jit(solution)/shard_map/all_to_all | solution.py:11
  98.0 10.1 %all-to-all-done.2 = bf16[32,16,256]{2,1,0:T(8,128)(2,1)S(1)} async-done(((bf16[32,16,256]{2,1,0:T(8,128)(2,1)}), bf16[32,16,256]{2,1,0:T(8,128)(2,1)S(1)}, u32[]{:S(2)}, u32[]{:S(2)}) %all-to-all-start.2) | async-done | bytes 262176 | tf_op jit(solution)/shard_map/all_to_all | solution.py:11
  109.4 8.2 %all-to-all-start.3 = ((bf16[8,512,128]{2,1,0:T(8,128)(2,1)}), bf16[8,512,128]{2,1,0:T(8,128)(2,1)S(1)}, u32[]{:S(2)}, u32[]{:S(2)}) async-start(bf16[8,512,128]{2,1,0:T(8,128)(2,1)} %broadcast_in_dim.40), calls=%async_computation.3 | async-start | bytes 2097152 | tf_op jit(solution)/shard_map/all_to_all | solution.py:11
  117.8 9.0 %reduce-window.16 = s32[32,8,128]{2,1,0:T(8,128)S(1)} reduce-window(s32[32,8,128]{2,1,0:T(8,128)S(1)} %fusion.43, s32[]{:T(128)} %constant.60.clone.1), window={size=1x1x128 pad=0_0x0_0x127_0}, to_apply=%region_9.10 | reduce-window | flops 4161536 | bytes 262148 | tf_op jit(solution)/shard_map/reduce-window.2
  127.7 4.3 %scatter_custom_fusion = s32[2048]{0:T(1024)S(1)} fusion(s32[1024]{0:T(1024)S(1)} %bitcast.121, s32[1024]{0:T(1024)S(1)} %add_select_fusion, s32[]{:T(128)} %constant.58.clone.1), kind=kCustom, calls=%fused_computation.86 | custom fusion | bytes 8196 | tf_op jit(solution)/shard_map/scatter | solution.py:81
  137.4 8.9 %all-to-all-done.4 = f32[32,1,512]{2,1,0:T(1,128)S(1)} async-done(((f32[32,1,512]{2,1,0:T(1,128)}), f32[32,1,512]{2,1,0:T(1,128)S(1)}, u32[]{:S(2)}, u32[]{:S(2)}) %all-to-all-start.4) | async-done | bytes 65568 | tf_op jit(solution)/shard_map/all_to_all | solution.py:11
  146.5 6.2 %gather_fusion = bf16[2048,128]{1,0:T(8,128)(2,1)S(1)} fusion(bf16[513,128]{1,0:T(8,128)(2,1)S(1)} %concatenate.10, s32[2048]{0:T(1024)S(1)} %fusion.52), kind=kCustom, calls=%fused_computation | custom fusion | bytes 1056768 | tf_op jit(solution)/shard_map/gather | solution.py:162
  152.8 12.0 %all_to_all.86 = bf16[32,8,128]{2,1,0:T(8,128)(2,1)S(1)} all-to-all(bf16[32,8,128]{2,1,0:T(8,128)(2,1)S(1)} %constant_dynamic-slice_fusion), channel_id=1, replica_groups=mesh['ep'=32,'tp'=8] {'ep'}, dimensions={0} | all-to-all | bytes 131072 | tf_op jit(solution)/shard_map/all_to_all | solution.py:165
  164.8 16.2 %all_gather.3 = bf16[1,64,4096]{2,1,0:T(8,128)(2,1)S(1)} all-gather(bf16[1,8,4096]{2,1,0:T(8,128)(2,1)S(1)} %bitcast.112), channel_id=1, replica_groups=mesh['ep'=32,'tp'=8] {'tp'}, dimensions={1}, use_global_device_ids=true | all-gather | bytes 589824 | tf_op jit(solution)/shard_map/all_gather | solution.py:166
  188.9 8.0 %all-to-all-done.6 = bf16[8,1,8,4096]{3,2,1,0:T(8,128)(2,1)S(1)} async-done(((bf16[8,1,8,4096]{3,2,1,0:T(8,128)(2,1)}), bf16[8,1,8,4096]{3,2,1,0:T(8,128)(2,1)S(1)}, u32[]{:S(2)}, u32[]{:S(2)}) %all-to-all-start.6) | async-done | bytes 524320 | tf_op jit(solution)/shard_map/all_to_all | solution.py:26
  196.9 4.8 %all-to-all-start.9 = ((bf16[32,16,1024]{2,1,0:T(8,128)(2,1)}), bf16[32,16,1024]{2,1,0:T(8,128)(2,1)}, u32[]{:S(2)}, u32[]{:S(2)}) async-start(bf16[32,16,1024]{2,1,0:T(8,128)(2,1)} %bitcast.28), calls=%async_computation.9 | async-start | bytes 2097152 | tf_op jit(solution)/shard_map/all_to_all | solution.py:26
  205.1 23.4 %reduce.9 = bf16[4096,8]{1,0:T(8,128)(2,1)} reduce(bf16[4096,1,8]{2,1,0:T(2,128)(2,1)S(1)} %bitcast.103, bf16[]{:T(256)} %broadcast.165), dimensions={1}, to_apply=%bitcast.86.reduce_sub_computation | reduce | bytes 131074
  231.6 9.1 %all-to-all-start.7 = ((bf16[32,2,512]{2,1,0:T(2,128)(2,1)}), bf16[32,2,512]{2,1,0:T(2,128)(2,1)S(1)}, u32[]{:S(2)}, u32[]{:S(2)}) async-start(bf16[32,2,512]{2,1,0:T(2,128)(2,1)} %reshape.282), calls=%async_computation.7 | async-start | bytes 131072 | tf_op jit(solution)/shard_map/all_to_all | solution.py:169
  242.2 7.4 %all-to-all-done.7 = bf16[32,2,512]{2,1,0:T(2,128)(2,1)S(1)} async-done(((bf16[32,2,512]{2,1,0:T(2,128)(2,1)}), bf16[32,2,512]{2,1,0:T(2,128)(2,1)S(1)}, u32[]{:S(2)}, u32[]{:S(2)}) %all-to-all-start.7) | async-done | bytes 65568 | tf_op jit(solution)/shard_map/all_to_all | solution.py:169
  250.4 4.6 %all-to-all-start.10 = ((bf16[32,16,512]{2,1,0:T(8,128)(2,1)}), bf16[32,16,512]{2,1,0:T(8,128)(2,1)}, u32[]{:S(2)}, u32[]{:S(2)}) async-start(bf16[32,16,512]{2,1,0:T(8,128)(2,1)} %broadcast_in_dim.46), calls=%async_computation.10 | async-start | bytes 1048576 | tf_op jit(solution)/shard_map/all_to_all | solution.py:11
  259.8 9.4 %all-to-all-done.10 = bf16[32,16,512]{2,1,0:T(8,128)(2,1)} async-done(((bf16[32,16,512]{2,1,0:T(8,128)(2,1)}), bf16[32,16,512]{2,1,0:T(8,128)(2,1)}, u32[]{:S(2)}, u32[]{:S(2)}) %all-to-all-start.10) | async-done | bytes 524320 | tf_op jit(solution)/shard_map/all_to_all | solution.py:11
  270.1 8.2 %all-to-all-start.8 = ((bf16[8,32,8,128]{3,2,1,0:T(8,128)(2,1)}), bf16[8,32,8,128]{3,2,1,0:T(8,128)(2,1)S(1)}, u32[]{:S(2)}, u32[]{:S(2)}) async-start(bf16[8,32,8,128]{3,2,1,0:T(8,128)(2,1)} %broadcast_in_dim.45), calls=%async_computation.8 | async-start | bytes 1048576 | tf_op jit(solution)/shard_map/all_to_all | solution.py:11
  279.6 8.0 %all-to-all-done.8 = bf16[8,32,8,128]{3,2,1,0:T(8,128)(2,1)S(1)} async-done(((bf16[8,32,8,128]{3,2,1,0:T(8,128)(2,1)}), bf16[8,32,8,128]{3,2,1,0:T(8,128)(2,1)S(1)}, u32[]{:S(2)}, u32[]{:S(2)}) %all-to-all-start.8) | async-done | bytes 524320 | tf_op jit(solution)/shard_map/all_to_all | solution.py:11
  288.8 4.4 %all-to-all-start.11 = ((bf16[8,512,128]{2,1,0:T(8,128)(2,1)}), bf16[8,512,128]{2,1,0:T(8,128)(2,1)S(1)}, u32[]{:S(2)}, u32[]{:S(2)}) async-start(bf16[8,512,128]{2,1,0:T(8,128)(2,1)} %broadcast_in_dim.47), calls=%async_computation.11 | async-start | bytes 2097152 | tf_op jit(solution)/shard_map/all_to_all | solution.py:11
  301.8 6.4 %all-to-all-done.11 = bf16[8,512,128]{2,1,0:T(8,128)(2,1)S(1)} async-done(((bf16[8,512,128]{2,1,0:T(8,128)(2,1)}), bf16[8,512,128]{2,1,0:T(8,128)(2,1)S(1)}, u32[]{:S(2)}, u32[]{:S(2)}) %all-to-all-start.11) | async-done | bytes 1048608 | tf_op jit(solution)/shard_map/all_to_all | solution.py:11
  (103 shorter events, 54.9 us)
Async XLA Ops:
  0.6 181.9 %copy-start = (bf16[1,128,4096]{2,1,0:T(8,128)(2,1)S(1)}, bf16[1,128,4096]{2,1,0:T(8,128)(2,1)}, u32[]{:S(2)}) copy-start(bf16[1,128,4096]{2,1,0:T(8,128)(2,1)} %param.37) | copy-start | bytes 3145732
  24.5 18.8 %all-to-all-start.1 = ((bf16[32,16,512]{2,1,0:T(8,128)(2,1)}), bf16[32,16,512]{2,1,0:T(8,128)(2,1)S(1)}, u32[]{:S(2)}, u32[]{:S(2)}) async-start(bf16[32,16,512]{2,1,0:T(8,128)(2,1)} %bitcast), calls=%async_computation.1 | async-start | bytes 1048576 | tf_op jit(solution)/shard_map/all_to_all | solution.py:26
  46.8 43.6 %copy-start.8 = (f32[256]{0:T(256)S(1)}, f32[256]{0:T(256)}, u32[]{:S(2)}) copy-start(f32[256]{0:T(256)} %param.31) | copy-start | bytes 3076
  46.8 50.8 %copy-start.6 = (s32[512,2]{0,1:T(2,128)S(1)}, s32[512,2]{0,1:T(2,128)}, u32[]{:S(2)}) copy-start(s32[512,2]{0,1:T(2,128)} %param.33) | copy-start | bytes 12292
  46.9 61.1 %copy-start.5 = (bf16[256,128]{1,0:T(8,128)(2,1)S(1)}, bf16[256,128]{1,0:T(8,128)(2,1)}, u32[]{:S(2)}) copy-start(bf16[256,128]{1,0:T(8,128)(2,1)} %param.30) | copy-start | bytes 196612
  90.5 42.2 %copy-start.1 = (bf16[512,128]{1,0:T(8,128)(2,1)S(1)}, bf16[512,128]{1,0:T(8,128)(2,1)}, u32[]{:S(2)}) copy-start(bf16[512,128]{1,0:T(8,128)(2,1)} %param.21) | copy-start | bytes 393220
  91.3 55.1 %copy-start.9 = (f32[128]{0:T(128)S(1)}, f32[128]{0:T(128)}, u32[]{:S(2)}) copy-start(f32[128]{0:T(128)} %param.32) | copy-start | bytes 1540
  91.3 16.7 %all-to-all-start.2 = ((bf16[32,16,256]{2,1,0:T(8,128)(2,1)}), bf16[32,16,256]{2,1,0:T(8,128)(2,1)S(1)}, u32[]{:S(2)}, u32[]{:S(2)}) async-start(bf16[32,16,256]{2,1,0:T(8,128)(2,1)} %broadcast_in_dim.39), calls=%async_computation.2 | async-start | bytes 524288 | tf_op jit(solution)/shard_map/all_to_all | solution.py:11
  109.4 23.2 %all-to-all-start.3 = ((bf16[8,512,128]{2,1,0:T(8,128)(2,1)}), bf16[8,512,128]{2,1,0:T(8,128)(2,1)S(1)}, u32[]{:S(2)}, u32[]{:S(2)}) async-start(bf16[8,512,128]{2,1,0:T(8,128)(2,1)} %broadcast_in_dim.40), calls=%async_computation.3 | async-start | bytes 2097152 | tf_op jit(solution)/shard_map/all_to_all | solution.py:11
  132.7 49.8 %copy-start.2 = (bf16[1,4096,128]{2,1,0:T(8,128)(2,1)S(1)}, bf16[1,4096,128]{2,1,0:T(8,128)(2,1)}, u32[]{:S(2)}) copy-start(bf16[1,4096,128]{2,1,0:T(8,128)(2,1)} %param.36) | copy-start | bytes 3145732
  133.6 12.7 %all-to-all-start.4 = ((f32[32,1,512]{2,1,0:T(1,128)}), f32[32,1,512]{2,1,0:T(1,128)S(1)}, u32[]{:S(2)}, u32[]{:S(2)}) async-start(f32[32,1,512]{2,1,0:T(1,128)} %broadcast_in_dim.41), calls=%async_computation.4 | async-start | bytes 131072 | tf_op jit(solution)/shard_map/all_to_all | solution.py:11
  152.7 34.8 %copy-start.3 = (bf16[128,512]{1,0:T(8,128)(2,1)S(1)}, bf16[128,512]{1,0:T(8,128)(2,1)}, u32[]{:S(2)}) copy-start(bf16[128,512]{1,0:T(8,128)(2,1)} %param.39) | copy-start | bytes 393220
  152.7 34.8 %copy-start.4 = (bf16[128,512]{1,0:T(8,128)(2,1)S(1)}, bf16[128,512]{1,0:T(8,128)(2,1)}, u32[]{:S(2)}) copy-start(bf16[128,512]{1,0:T(8,128)(2,1)} %param.38) | copy-start | bytes 393220
  183.9 12.9 %all-to-all-start.6 = ((bf16[8,1,8,4096]{3,2,1,0:T(8,128)(2,1)}), bf16[8,1,8,4096]{3,2,1,0:T(8,128)(2,1)S(1)}, u32[]{:S(2)}, u32[]{:S(2)}) async-start(bf16[8,1,8,4096]{3,2,1,0:T(8,128)(2,1)} %fusion), calls=%async_computation.6 | async-start | bytes 1048576 | tf_op jit(solution)/shard_map/all_to_all | solution.py:26
  196.9 34.7 %all-to-all-start.9 = ((bf16[32,16,1024]{2,1,0:T(8,128)(2,1)}), bf16[32,16,1024]{2,1,0:T(8,128)(2,1)}, u32[]{:S(2)}, u32[]{:S(2)}) async-start(bf16[32,16,1024]{2,1,0:T(8,128)(2,1)} %bitcast.28), calls=%async_computation.9 | async-start | bytes 2097152 | tf_op jit(solution)/shard_map/all_to_all | solution.py:26
  231.6 18.0 %all-to-all-start.7 = ((bf16[32,2,512]{2,1,0:T(2,128)(2,1)}), bf16[32,2,512]{2,1,0:T(2,128)(2,1)S(1)}, u32[]{:S(2)}, u32[]{:S(2)}) async-start(bf16[32,2,512]{2,1,0:T(2,128)(2,1)} %reshape.282), calls=%async_computation.7 | async-start | bytes 131072 | tf_op jit(solution)/shard_map/all_to_all | solution.py:169
  250.4 18.8 %all-to-all-start.10 = ((bf16[32,16,512]{2,1,0:T(8,128)(2,1)}), bf16[32,16,512]{2,1,0:T(8,128)(2,1)}, u32[]{:S(2)}, u32[]{:S(2)}) async-start(bf16[32,16,512]{2,1,0:T(8,128)(2,1)} %broadcast_in_dim.46), calls=%async_computation.10 | async-start | bytes 1048576 | tf_op jit(solution)/shard_map/all_to_all | solution.py:11
  257.9 35.4 %copy-start.7 = (f32[512,2]{0,1:T(2,128)S(1)}, f32[512,2]{0,1:T(2,128)}, u32[]{:S(2)}) copy-start(f32[512,2]{0,1:T(2,128)} %param.34) | copy-start | bytes 12292
  270.1 17.6 %all-to-all-start.8 = ((bf16[8,32,8,128]{3,2,1,0:T(8,128)(2,1)}), bf16[8,32,8,128]{3,2,1,0:T(8,128)(2,1)S(1)}, u32[]{:S(2)}, u32[]{:S(2)}) async-start(bf16[8,32,8,128]{3,2,1,0:T(8,128)(2,1)} %broadcast_in_dim.45), calls=%async_computation.8 | async-start | bytes 1048576 | tf_op jit(solution)/shard_map/all_to_all | solution.py:11
  279.6 28.7 %copy-start.10 = (f32[128]{0:T(128)S(1)}, f32[128]{0:T(128)}, u32[]{:S(2)}) copy-start(f32[128]{0:T(128)} %param.41) | copy-start | bytes 1540
  288.8 19.4 %all-to-all-start.11 = ((bf16[8,512,128]{2,1,0:T(8,128)(2,1)}), bf16[8,512,128]{2,1,0:T(8,128)(2,1)S(1)}, u32[]{:S(2)}, u32[]{:S(2)}) async-start(bf16[8,512,128]{2,1,0:T(8,128)(2,1)} %broadcast_in_dim.47), calls=%async_computation.11 | async-start | bytes 2097152 | tf_op jit(solution)/shard_map/all_to_all | solution.py:11
where the time goes:
time: 310 us; the launch traced here: 309 us
  other arithmetic  81 us (26%)
  waiting for transfers between devices  72.8 us (23%)
  starting transfers between devices  57.1 us (18%)
  blocking collectives  48.7 us (16%)
  local copies, waits for them, and re-layouts  33.7 us (11%)
  matrix products  14.7 us (5%)
    another operation x5, other arithmetic  48.8 us
    all_to_all x6, waiting for transfers between devices, sent_to_all(): lax.all_to_all(jnp.broadcast_to(x[None], (size, *x.shape)), axis, 0, 0, t...  43.3 us
    all_to_all x6, starting transfers between devices, sent_to_all(): lax.all_to_all(jnp.broadcast_to(x[None], (size, *x.shape)), axis, 0, 0, t...  35.6 us
    unnamed x1, other arithmetic  23.4 us
    all_to_all x3, waiting for transfers between devices, sent_and_summed(): lax.all_to_all(blocks, axis, split_axis=0, concat_axis=0, tiled=True)  22.1 us
    all_to_all x1, blocking collectives, sent_to_all(): lax.all_to_all(jnp.broadcast_to(x[None], (size, *x.shape)), axis, 0, 0, t...  20.5 us
    all_gather x1, blocking collectives, per_device(): gathered = lax.all_gather(arrived, 'tp', axis=1, tiled=True)  16.2 us
    all_to_all x3, starting transfers between devices, sent_and_summed(): lax.all_to_all(blocks, axis, split_axis=0, concat_axis=0, tiled=True)  12.3 us
  transfers between devices with their start and end apart: 10, of which 9 were waited for; matrix products, arithmetic and copies ran while one was open for 20% of the time, Pallas kernels for 0%

commit v1 on v0

--- a/solution.py
+++ b/solution.py
@@ -163,7 +163,9 @@
     slot_share = capacity // lax.axis_size("tp")
     own_slots = lax.dynamic_slice_in_dim(outgoing, lax.axis_index("tp") * slot_share, slot_share, 1)
     arrived = lax.all_to_all(own_slots, "ep", split_axis=0, concat_axis=2, tiled=True)
-    gathered = lax.all_gather(arrived, "tp", axis=1, tiled=True)
+    num = lax.axis_size("tp")
+    local_now = jnp.tile(arrived, [num if t == 1 else 1 for t in range(arrived.ndim)])
+    gathered = lax.all_to_all(local_now, "tp", concat_axis=1, tiled=True, split_axis=1)
     partial_value = expert_terms(gathered, expert_gate, expert_up, expert_down)
     summed = sent_and_summed(partial_value.astype(jnp.bfloat16), "tp", 1).astype(jnp.bfloat16)
     came_back = lax.all_to_all(summed, "ep", split_axis=2, concat_axis=0, tiled=True)

time: 310 us -> 319 us (1.029)
  other arithmetic: 81 us -> 84.8 us
    all_gather x1 -> x0, blocking collectives: 16.2 us -> none  [per_device(): gathered = lax.all_gather(arrived, 'tp', axis=1, tiled=True)]
    all_to_all x0 -> x1, blocking collectives: none -> 15.8 us  [per_device(): lax.all_to_all(local_now, 'tp', concat_axis=1, tiled=True, split_axis=1)]
    unnamed x1 -> x2, other arithmetic: 23.4 us -> 27.2 us
where the time goes in v1:
time: 319 us; the launch traced here: 317 us
  other arithmetic  84.8 us (27%)
  waiting for transfers between devices  72.8 us (23%)
  starting transfers between devices  57.8 us (18%)
  blocking collectives  48.2 us (15%)
  local copies, waits for them, and re-layouts  35.9 us (11%)
  matrix products  16.8 us (5%)
    another operation x5, other arithmetic  48.8 us
    all_to_all x6, waiting for transfers between devices, sent_to_all(): lax.all_to_all(jnp.broadcast_to(x[None], (size, *x.shape)), axis, 0, 0, t...  43.3 us
    all_to_all x6, starting transfers between devices, sent_to_all(): lax.all_to_all(jnp.broadcast_to(x[None], (size, *x.shape)), axis, 0, 0, t...  35.6 us
    unnamed x2, other arithmetic  27.2 us
    all_to_all x3, waiting for transfers between devices, sent_and_summed(): lax.all_to_all(blocks, axis, split_axis=0, concat_axis=0, tiled=True)  22.1 us
    all_to_all x1, blocking collectives, sent_to_all(): lax.all_to_all(jnp.broadcast_to(x[None], (size, *x.shape)), axis, 0, 0, t...  20.5 us
    all_to_all x1, blocking collectives, per_device(): lax.all_to_all(local_now, 'tp', concat_axis=1, tiled=True, split_axis=1)  15.8 us
    all_to_all x3, starting transfers between devices, sent_and_summed(): lax.all_to_all(blocks, axis, split_axis=0, concat_axis=0, tiled=True)  13.2 us
  transfers between devices with their start and end apart: 10, of which 9 were waited for; matrix products, arithmetic and copies ran while one was open for 20% of the time, Pallas kernels for 0%

profile of v1, /device:TPU:1, one launch (start us, length us, event | category | flops | bytes accessed | tf_op | source)
XLA Modules:
  0.0 317.4 jit_solution(1583011930982867396)
XLA Ops:
  1.8 20.5 %all_to_all.87 = f32[32,1,512]{2,1,0:T(1,128)S(1)} all-to-all(f32[32,1,512]{2,1,0:T(1,128)S(1)} %broadcast_in_dim.37), channel_id=1, replica_groups=mesh['ep'=32,'tp'=8] {'ep'}, dimensions={0} | all-to-all | bytes 131072 | tf_op jit(solution)/shard_map/all_to_all | solution.py:11
  29.1 14.2 %all-to-all-done.1 = bf16[32,16,512]{2,1,0:T(8,128)(2,1)S(1)} async-done(((bf16[32,16,512]{2,1,0:T(8,128)(2,1)}), bf16[32,16,512]{2,1,0:T(8,128)(2,1)S(1)}, u32[]{:S(2)}, u32[]{:S(2)}) %all-to-all-start.1) | async-done | bytes 524320 | tf_op jit(solution)/shard_map/all_to_all | solution.py:26
  47.0 39.6 %reduce-window.14 = f32[16,1,2,8,128]{4,3,2,1,0:T(8,128)S(1)} reduce-window(f32[16,1,2,8,128]{4,3,2,1,0:T(8,128)S(1)} %bitcast.120, f32[]{:T(128)} %constant.52.clone.1), window={size=1x1x1x1x128 pad=0_0x0_0x0_0x0_0x0_127}, to_apply=%region_3.4 | reduce-window | flops 4161536 | bytes 262148 | tf_op jit(solution)/shard_map/reduce-window
  91.3 6.3 %all-to-all-start.2 = ((bf16[32,16,256]{2,1,0:T(8,128)(2,1)}), bf16[32,16,256]{2,1,0:T(8,128)(2,1)S(1)}, u32[]{:S(2)}, u32[]{:S(2)}) async-start(bf16[32,16,256]{2,1,0:T(8,128)(2,1)} %broadcast_in_dim.39), calls=%async_computation.2 | async-start | bytes 524288 | tf_op jit(solution)/shard_map/all_to_all | solution.py:11
  98.0 10.1 %all-to-all-done.2 = bf16[32,16,256]{2,1,0:T(8,128)(2,1)S(1)} async-done(((bf16[32,16,256]{2,1,0:T(8,128)(2,1)}), bf16[32,16,256]{2,1,0:T(8,128)(2,1)S(1)}, u32[]{:S(2)}, u32[]{:S(2)}) %all-to-all-start.2) | async-done | bytes 262176 | tf_op jit(solution)/shard_map/all_to_all | solution.py:11
  109.4 8.2 %all-to-all-start.3 = ((bf16[8,512,128]{2,1,0:T(8,128)(2,1)}), bf16[8,512,128]{2,1,0:T(8,128)(2,1)S(1)}, u32[]{:S(2)}, u32[]{:S(2)}) async-start(bf16[8,512,128]{2,1,0:T(8,128)(2,1)} %broadcast_in_dim.40), calls=%async_computation.3 | async-start | bytes 2097152 | tf_op jit(solution)/shard_map/all_to_all | solution.py:11
  117.8 9.0 %reduce-window.16 = s32[32,8,128]{2,1,0:T(8,128)S(1)} reduce-window(s32[32,8,128]{2,1,0:T(8,128)S(1)} %fusion.46, s32[]{:T(128)} %constant.60.clone.1), window={size=1x1x128 pad=0_0x0_0x127_0}, to_apply=%region_9.10 | reduce-window | flops 4161536 | bytes 262148 | tf_op jit(solution)/shard_map/reduce-window.2
  127.7 4.3 %scatter_custom_fusion = s32[2048]{0:T(1024)S(1)} fusion(s32[1024]{0:T(1024)S(1)} %bitcast.130, s32[1024]{0:T(1024)S(1)} %add_select_fusion, s32[]{:T(128)} %constant.58.clone.1), kind=kCustom, calls=%fused_computation.89 | custom fusion | bytes 8196 | tf_op jit(solution)/shard_map/scatter | solution.py:81
  137.4 8.9 %all-to-all-done.4 = f32[32,1,512]{2,1,0:T(1,128)S(1)} async-done(((f32[32,1,512]{2,1,0:T(1,128)}), f32[32,1,512]{2,1,0:T(1,128)S(1)}, u32[]{:S(2)}, u32[]{:S(2)}) %all-to-all-start.4) | async-done | bytes 65568 | tf_op jit(solution)/shard_map/all_to_all | solution.py:11
  146.5 6.2 %gather_fusion = bf16[2048,128]{1,0:T(8,128)(2,1)S(1)} fusion(bf16[513,128]{1,0:T(8,128)(2,1)S(1)} %concatenate.10, s32[2048]{0:T(1024)S(1)} %fusion.55), kind=kCustom, calls=%fused_computation | custom fusion | bytes 1056768 | tf_op jit(solution)/shard_map/gather | solution.py:162
  152.8 11.9 %all_to_all.88 = bf16[32,8,128]{2,1,0:T(8,128)(2,1)S(1)} all-to-all(bf16[32,8,128]{2,1,0:T(8,128)(2,1)S(1)} %constant_dynamic-slice_fusion), channel_id=1, replica_groups=mesh['ep'=32,'tp'=8] {'ep'}, dimensions={0} | all-to-all | bytes 131072 | tf_op jit(solution)/shard_map/all_to_all | solution.py:165
  170.7 15.8 %all_to_all.89 = bf16[8,2,16384]{2,1,0:T(2,128)(2,1)S(1)} all-to-all(bf16[8,2,16384]{2,1,0:T(2,128)(2,1)S(1)} %reshape.289), channel_id=1, replica_groups=mesh['ep'=32,'tp'=8] {'tp'}, dimensions={0} | all-to-all | bytes 1048576 | tf_op jit(solution)/shard_map/all_to_all | solution.py:168
  192.1 4.4 %all-to-all-start.7 = ((bf16[8,1,8,4096]{3,2,1,0:T(8,128)(2,1)}), bf16[8,1,8,4096]{3,2,1,0:T(8,128)(2,1)S(1)}, u32[]{:S(2)}, u32[]{:S(2)}) async-start(bf16[8,1,8,4096]{3,2,1,0:T(8,128)(2,1)} %fusion), calls=%async_computation.7 | async-start | bytes 1048576 | tf_op jit(solution)/shard_map/all_to_all | solution.py:26
  197.9 8.0 %all-to-all-done.7 = bf16[8,1,8,4096]{3,2,1,0:T(8,128)(2,1)S(1)} async-done(((bf16[8,1,8,4096]{3,2,1,0:T(8,128)(2,1)}), bf16[8,1,8,4096]{3,2,1,0:T(8,128)(2,1)S(1)}, u32[]{:S(2)}, u32[]{:S(2)}) %all-to-all-start.7) | async-done | bytes 524320 | tf_op jit(solution)/shard_map/all_to_all | solution.py:26
  205.9 4.9 %all-to-all-start.10 = ((bf16[32,16,1024]{2,1,0:T(8,128)(2,1)}), bf16[32,16,1024]{2,1,0:T(8,128)(2,1)}, u32[]{:S(2)}, u32[]{:S(2)}) async-start(bf16[32,16,1024]{2,1,0:T(8,128)(2,1)} %bitcast.28), calls=%async_computation.10 | async-start | bytes 2097152 | tf_op jit(solution)/shard_map/all_to_all | solution.py:26
  213.6 23.4 %reduce.10 = bf16[4096,8]{1,0:T(8,128)(2,1)} reduce(bf16[4096,1,8]{2,1,0:T(2,128)(2,1)S(1)} %bitcast.109, bf16[]{:T(256)} %broadcast.168), dimensions={1}, to_apply=%bitcast.90.reduce_sub_computation | reduce | bytes 131074
  240.1 8.9 %all-to-all-start.8 = ((bf16[32,2,512]{2,1,0:T(2,128)(2,1)}), bf16[32,2,512]{2,1,0:T(2,128)(2,1)S(1)}, u32[]{:S(2)}, u32[]{:S(2)}) async-start(bf16[32,2,512]{2,1,0:T(2,128)(2,1)} %reshape.291), calls=%async_computation.8 | async-start | bytes 131072 | tf_op jit(solution)/shard_map/all_to_all | solution.py:171
  250.5 7.4 %all-to-all-done.8 = bf16[32,2,512]{2,1,0:T(2,128)(2,1)S(1)} async-done(((bf16[32,2,512]{2,1,0:T(2,128)(2,1)}), bf16[32,2,512]{2,1,0:T(2,128)(2,1)S(1)}, u32[]{:S(2)}, u32[]{:S(2)}) %all-to-all-start.8) | async-done | bytes 65568 | tf_op jit(solution)/shard_map/all_to_all | solution.py:171
  258.7 4.6 %all-to-all-start.11 = ((bf16[32,16,512]{2,1,0:T(8,128)(2,1)}), bf16[32,16,512]{2,1,0:T(8,128)(2,1)}, u32[]{:S(2)}, u32[]{:S(2)}) async-start(bf16[32,16,512]{2,1,0:T(8,128)(2,1)} %broadcast_in_dim.46), calls=%async_computation.11 | async-start | bytes 1048576 | tf_op jit(solution)/shard_map/all_to_all | solution.py:11
  268.1 9.4 %all-to-all-done.11 = bf16[32,16,512]{2,1,0:T(8,128)(2,1)} async-done(((bf16[32,16,512]{2,1,0:T(8,128)(2,1)}), bf16[32,16,512]{2,1,0:T(8,128)(2,1)}, u32[]{:S(2)}, u32[]{:S(2)}) %all-to-all-start.11) | async-done | bytes 524320 | tf_op jit(solution)/shard_map/all_to_all | solution.py:11
  278.4 8.2 %all-to-all-start.9 = ((bf16[8,32,8,128]{3,2,1,0:T(8,128)(2,1)}), bf16[8,32,8,128]{3,2,1,0:T(8,128)(2,1)S(1)}, u32[]{:S(2)}, u32[]{:S(2)}) async-start(bf16[8,32,8,128]{3,2,1,0:T(8,128)(2,1)} %broadcast_in_dim.45), calls=%async_computation.9 | async-start | bytes 1048576 | tf_op jit(solution)/shard_map/all_to_all | solution.py:11
  288.0 8.0 %all-to-all-done.9 = bf16[8,32,8,128]{3,2,1,0:T(8,128)(2,1)S(1)} async-done(((bf16[8,32,8,128]{3,2,1,0:T(8,128)(2,1)}), bf16[8,32,8,128]{3,2,1,0:T(8,128)(2,1)S(1)}, u32[]{:S(2)}, u32[]{:S(2)}) %all-to-all-start.9) | async-done | bytes 524320 | tf_op jit(solution)/shard_map/all_to_all | solution.py:11
  297.1 4.4 %all-to-all-start.12 = ((bf16[8,512,128]{2,1,0:T(8,128)(2,1)}), bf16[8,512,128]{2,1,0:T(8,128)(2,1)S(1)}, u32[]{:S(2)}, u32[]{:S(2)}) async-start(bf16[8,512,128]{2,1,0:T(8,128)(2,1)} %broadcast_in_dim.47), calls=%async_computation.12 | async-start | bytes 2097152 | tf_op jit(solution)/shard_map/all_to_all | solution.py:11
  310.1 6.4 %all-to-all-done.12 = bf16[8,512,128]{2,1,0:T(8,128)(2,1)S(1)} async-done(((bf16[8,512,128]{2,1,0:T(8,128)(2,1)}), bf16[8,512,128]{2,1,0:T(8,128)(2,1)S(1)}, u32[]{:S(2)}, u32[]{:S(2)}) %all-to-all-start.12) | async-done | bytes 1048608 | tf_op jit(solution)/shard_map/all_to_all | solution.py:11
  (106 shorter events, 63.3 us)
Async XLA Ops:
  0.6 188.4 %copy-start = (bf16[1,128,4096]{2,1,0:T(8,128)(2,1)S(1)}, bf16[1,128,4096]{2,1,0:T(8,128)(2,1)}, u32[]{:S(2)}) copy-start(bf16[1,128,4096]{2,1,0:T(8,128)(2,1)} %param.37) | copy-start | bytes 3145732
  24.5 18.8 %all-to-all-start.1 = ((bf16[32,16,512]{2,1,0:T(8,128)(2,1)}), bf16[32,16,512]{2,1,0:T(8,128)(2,1)S(1)}, u32[]{:S(2)}, u32[]{:S(2)}) async-start(bf16[32,16,512]{2,1,0:T(8,128)(2,1)} %bitcast), calls=%async_computation.1 | async-start | bytes 1048576 | tf_op jit(solution)/shard_map/all_to_all | solution.py:26
  46.8 43.6 %copy-start.7 = (f32[256]{0:T(256)S(1)}, f32[256]{0:T(256)}, u32[]{:S(2)}) copy-start(f32[256]{0:T(256)} %param.31) | copy-start | bytes 3076
  46.8 50.8 %copy-start.5 = (s32[512,2]{0,1:T(2,128)S(1)}, s32[512,2]{0,1:T(2,128)}, u32[]{:S(2)}) copy-start(s32[512,2]{0,1:T(2,128)} %param.33) | copy-start | bytes 12292
  46.9 61.1 %copy-start.4 = (bf16[256,128]{1,0:T(8,128)(2,1)S(1)}, bf16[256,128]{1,0:T(8,128)(2,1)}, u32[]{:S(2)}) copy-start(bf16[256,128]{1,0:T(8,128)(2,1)} %param.30) | copy-start | bytes 196612
  90.5 42.2 %copy-start.1 = (bf16[512,128]{1,0:T(8,128)(2,1)S(1)}, bf16[512,128]{1,0:T(8,128)(2,1)}, u32[]{:S(2)}) copy-start(bf16[512,128]{1,0:T(8,128)(2,1)} %param.21) | copy-start | bytes 393220
  91.3 55.1 %copy-start.8 = (f32[128]{0:T(128)S(1)}, f32[128]{0:T(128)}, u32[]{:S(2)}) copy-start(f32[128]{0:T(128)} %param.32) | copy-start | bytes 1540
  91.3 16.7 %all-to-all-start.2 = ((bf16[32,16,256]{2,1,0:T(8,128)(2,1)}), bf16[32,16,256]{2,1,0:T(8,128)(2,1)S(1)}, u32[]{:S(2)}, u32[]{:S(2)}) async-start(bf16[32,16,256]{2,1,0:T(8,128)(2,1)} %broadcast_in_dim.39), calls=%async_computation.2 | async-start | bytes 524288 | tf_op jit(solution)/shard_map/all_to_all | solution.py:11
  109.4 23.2 %all-to-all-start.3 = ((bf16[8,512,128]{2,1,0:T(8,128)(2,1)}), bf16[8,512,128]{2,1,0:T(8,128)(2,1)S(1)}, u32[]{:S(2)}, u32[]{:S(2)}) async-start(bf16[8,512,128]{2,1,0:T(8,128)(2,1)} %broadcast_in_dim.40), calls=%async_computation.3 | async-start | bytes 2097152 | tf_op jit(solution)/shard_map/all_to_all | solution.py:11
  133.5 12.7 %all-to-all-start.4 = ((f32[32,1,512]{2,1,0:T(1,128)}), f32[32,1,512]{2,1,0:T(1,128)S(1)}, u32[]{:S(2)}, u32[]{:S(2)}) async-start(f32[32,1,512]{2,1,0:T(1,128)} %broadcast_in_dim.41), calls=%async_computation.4 | async-start | bytes 131072 | tf_op jit(solution)/shard_map/all_to_all | solution.py:11
  170.7 25.8 %copy-start.2 = (bf16[128,512]{1,0:T(8,128)(2,1)S(1)}, bf16[128,512]{1,0:T(8,128)(2,1)}, u32[]{:S(2)}) copy-start(bf16[128,512]{1,0:T(8,128)(2,1)} %param.39) | copy-start | bytes 393220
  170.7 25.8 %copy-start.3 = (bf16[128,512]{1,0:T(8,128)(2,1)S(1)}, bf16[128,512]{1,0:T(8,128)(2,1)}, u32[]{:S(2)}) copy-start(bf16[128,512]{1,0:T(8,128)(2,1)} %param.38) | copy-start | bytes 393220
  192.1 13.8 %all-to-all-start.7 = ((bf16[8,1,8,4096]{3,2,1,0:T(8,128)(2,1)}), bf16[8,1,8,4096]{3,2,1,0:T(8,128)(2,1)S(1)}, u32[]{:S(2)}, u32[]{:S(2)}) async-start(bf16[8,1,8,4096]{3,2,1,0:T(8,128)(2,1)} %fusion), calls=%async_computation.7 | async-start | bytes 1048576 | tf_op jit(solution)/shard_map/all_to_all | solution.py:26
  205.9 34.3 %all-to-all-start.10 = ((bf16[32,16,1024]{2,1,0:T(8,128)(2,1)}), bf16[32,16,1024]{2,1,0:T(8,128)(2,1)}, u32[]{:S(2)}, u32[]{:S(2)}) async-start(bf16[32,16,1024]{2,1,0:T(8,128)(2,1)} %bitcast.28), calls=%async_computation.10 | async-start | bytes 2097152 | tf_op jit(solution)/shard_map/all_to_all | solution.py:26
  240.1 17.8 %all-to-all-start.8 = ((bf16[32,2,512]{2,1,0:T(2,128)(2,1)}), bf16[32,2,512]{2,1,0:T(2,128)(2,1)S(1)}, u32[]{:S(2)}, u32[]{:S(2)}) async-start(bf16[32,2,512]{2,1,0:T(2,128)(2,1)} %reshape.291), calls=%async_computation.8 | async-start | bytes 131072 | tf_op jit(solution)/shard_map/all_to_all | solution.py:171
  258.7 18.8 %all-to-all-start.11 = ((bf16[32,16,512]{2,1,0:T(8,128)(2,1)}), bf16[32,16,512]{2,1,0:T(8,128)(2,1)}, u32[]{:S(2)}, u32[]{:S(2)}) async-start(bf16[32,16,512]{2,1,0:T(8,128)(2,1)} %broadcast_in_dim.46), calls=%async_computation.11 | async-start | bytes 1048576 | tf_op jit(solution)/shard_map/all_to_all | solution.py:11
  266.2 35.4 %copy-start.6 = (f32[512,2]{0,1:T(2,128)S(1)}, f32[512,2]{0,1:T(2,128)}, u32[]{:S(2)}) copy-start(f32[512,2]{0,1:T(2,128)} %param.34) | copy-start | bytes 12292
  278.4 17.6 %all-to-all-start.9 = ((bf16[8,32,8,128]{3,2,1,0:T(8,128)(2,1)}), bf16[8,32,8,128]{3,2,1,0:T(8,128)(2,1)S(1)}, u32[]{:S(2)}, u32[]{:S(2)}) async-start(bf16[8,32,8,128]{3,2,1,0:T(8,128)(2,1)} %broadcast_in_dim.45), calls=%async_computation.9 | async-start | bytes 1048576 | tf_op jit(solution)/shard_map/all_to_all | solution.py:11
  287.9 28.7 %copy-start.9 = (f32[128]{0:T(128)S(1)}, f32[128]{0:T(128)}, u32[]{:S(2)}) copy-start(f32[128]{0:T(128)} %param.41) | copy-start | bytes 1540
  297.1 19.4 %all-to-all-start.12 = ((bf16[8,512,128]{2,1,0:T(8,128)(2,1)}), bf16[8,512,128]{2,1,0:T(8,128)(2,1)S(1)}, u32[]{:S(2)}, u32[]{:S(2)}) async-start(bf16[8,512,128]{2,1,0:T(8,128)(2,1)} %broadcast_in_dim.47), calls=%async_computation.12 | async-start | bytes 2097152 | tf_op jit(solution)/shard_map/all_to_all | solution.py:11
